TPU v7x, 128 devices: a 2x2x16 block of a 8x8x16 slice. The times are simulated.
128 devices in a mesh: grp: 4 (over y, x), ep: 32 (over z, core).
Axes of the slice: x: 2, y: 2, z: 16, core: 2. Of those that a mesh axis runs over, the one named last changes fastest.
The devices are a block of a 8x8x16 slice.
Arguments:
- tokens: bfloat16 [4096, 2048], P(('grp', 'ep')), parts along dimension 0, may hold values from -6 to 6
- routes: int32 [4096, 4], P(('grp', 'ep')), parts along dimension 0, may hold values from 0 to 31, all different within a row; in each aligned block of 32 rows (0 to 31, 32 to 63, ...) at most 8 rows name the same one
- route_logits: float32 [4096, 4], P(('grp', 'ep')), parts along dimension 0, may hold values from -4 to 4
- state_real: float32 [4096, 64, 64], P('grp', 'ep'), parts along dimension 0, may hold values from -4 to 4
- state_imag: float32 [4096, 64, 64], P('grp', 'ep'), parts along dimension 0, may hold values from -4 to 4
- gain_in: float32 [2048], replicated, may hold values from 0.1 to 1.9
- proj_in: bfloat16 [2048, 1024], P(None, 'ep'), may hold values from -0.125 to 0.125
- decay_rate: float32 [64, 64], P('ep'), may hold values from 0.05 to 2
- frequency: float32 [64, 64], P('ep'), may hold values from -4 to 4
- log_step: float32 [64], P('ep'), may hold values from -3 to 0
- input_real: float32 [64, 64, 16], P('ep'), may hold values from -1 to 1
- input_imag: float32 [64, 64, 16], P('ep'), may hold values from -1 to 1
- output_real: float32 [64, 16, 64], P('ep'), may hold values from -0.5 to 0.5
- output_imag: float32 [64, 16, 64], P('ep'), may hold values from -0.5 to 0.5
- skip_gain: float32 [64, 16], P('ep'), may hold values from -4 to 4
- proj_out: bfloat16 [1024, 2048], P('ep'), may hold values from -0.1875 to 0.1875
- gain_mid: float32 [2048], replicated, may hold values from 0.1 to 1.9
- expert_gate: bfloat16 [32, 2048, 1024], P('ep'), may hold values from -0.33007812 to 0.33007812
- expert_up: bfloat16 [32, 2048, 1024], P('ep'), may hold values from -0.33007812 to 0.33007812
- expert_down: bfloat16 [32, 1024, 2048], P('ep'), may hold values from -0.056152344 to 0.056152344
- dense_gate: bfloat16 [2048, 2048], P(None, 'ep'), may hold values from -0.125 to 0.125
- dense_up: bfloat16 [2048, 2048], P(None, 'ep'), may hold values from -0.125 to 0.125
- dense_down: bfloat16 [2048, 2048], P('ep'), may hold values from -0.125 to 0.125
- dense_mix: float32 [2048], P('ep'), may hold values from -0.39774758 to 0.39774758
Outputs:
- layer_out: bfloat16 [4096, 2048], P(('grp', 'ep')), parts along dimension 0
- state_real_new: float32 [4096, 64, 64], P('grp', 'ep'), parts along dimension 0
- state_imag_new: float32 [4096, 64, 64], P('grp', 'ep'), parts along dimension 0
There are 4 independent parts, one for each index of `grp`. A program takes and returns all parts, laid end to end along the dimension named above; an argument that names none is the same for every part. Nothing has to cross between parts.
Inputs may be any that keep to these rules, and one draw needn't show every extreme that they name: `routes`: each row names 4 different experts; among the rows of one device no expert is named more than 8 times, and in every draw some device names some expert exactly 8 times.
All inputs are finite; a program needn't handle non-finite values.
Results may differ from a plain program's by a relative error of at most 0.015.
Values may be sent and summed in bfloat16 or wider, within the bound.
A program may use at most 128 MiB of HBM per device.

v0:
```python
import jax
import jax.numpy as jnp
from jax import lax
from jax.sharding import Mesh
from jax.sharding import PartitionSpec as P

EP = ("ep_0", "ep_1")
GRP_EP = ("grp", "ep_0", "ep_1")
EPS = 1e-06
LIMIT = 7.0
ALPHA = 1.702


def copy_for_each(shard, axis):
    length = lax.axis_size(axis)
    return lax.all_to_all(
        jnp.broadcast_to(shard[None], (length, *shard.shape)), axis, 0, 0, tiled=True
    )


def of_everyone(shard, axis):
    return copy_for_each(shard, axis).sum(axis=0)


def reduced_to_own(blocks, axes, turns):
    lengths = [lax.axis_size(a) for a in axes]
    blocks = blocks.reshape(*lengths, *blocks.shape[1:])
    blocks = blocks.transpose(*turns, *range(len(axes), blocks.ndim))
    blocks = blocks.reshape(-1, *blocks.shape[len(axes) :])
    for k in turns:
        blocks = lax.psum_scatter(blocks, axes[k], scatter_dimension=0, tiled=True)
    return blocks[0]


def split_up(shard, dim, length):
    before, after = (shard.shape[:dim], shard.shape[dim + 1 :])
    return jnp.moveaxis(shard.reshape(*before, length, -1, *after), dim, 0)


def scatter_axes(shard, axes, turns, dim):
    length = lax.axis_size(axes)
    return reduced_to_own(split_up(shard, dim, length), axes, turns)


def rms_scale(values, gain_vec):
    return values * lax.rsqrt(jnp.mean(values * values, axis=-1, keepdims=True) + EPS) * gain_vec


def state_step(
    unit_rows,
    state_real,
    state_imag,
    decay_rate,
    frequency,
    log_step,
    input_real,
    input_imag,
    output_real,
    output_imag,
    skip_gain,
):
    seq_count = unit_rows.shape[0]
    groups, group_size = skip_gain.shape
    inputs = unit_rows.astype(jnp.float32).reshape(seq_count, groups, group_size)
    step_size = jnp.exp(log_step)[:, None]
    decay_part = -decay_rate
    magnitude = jnp.exp(decay_part * step_size)
    carry_real = magnitude * jnp.cos(frequency * step_size)
    carry_imag = magnitude * jnp.sin(frequency * step_size)
    denom = decay_part * decay_part + frequency * frequency
    feed_real = ((carry_real - 1.0) * decay_part + carry_imag * frequency) / denom
    feed_imag = (carry_imag * decay_part - (carry_real - 1.0) * frequency) / denom
    drive_real = jnp.einsum("sgp,gnp->sgn", inputs, input_real)
    drive_imag = jnp.einsum("sgp,gnp->sgn", inputs, input_imag)
    new_real = (
        carry_real * state_real
        - carry_imag * state_imag
        + feed_real * drive_real
        - feed_imag * drive_imag
    )
    new_imag = (
        carry_real * state_imag
        + carry_imag * state_real
        + feed_real * drive_imag
        + feed_imag * drive_real
    )
    readout = (
        jnp.einsum("gpn,sgn->sgp", output_real, new_real)
        - jnp.einsum("gpn,sgn->sgp", output_imag, new_imag)
        + skip_gain * inputs
    )
    branch = jax.nn.gelu(readout).reshape(seq_count, groups * group_size).astype(jnp.bfloat16)
    return (branch, new_real, new_imag)


def expert_apply(row_block, gate_weight, up_weight, down_weight):
    gated = jnp.minimum(jnp.dot(row_block, gate_weight, preferred_element_type=jnp.float32), LIMIT)
    upper = jnp.clip(
        jnp.dot(row_block, up_weight, preferred_element_type=jnp.float32), -LIMIT, LIMIT
    )
    activated = ((upper + 1.0) * gated * jax.nn.sigmoid(ALPHA * gated)).astype(jnp.bfloat16)
    return jnp.dot(activated, down_weight, preferred_element_type=jnp.float32).astype(jnp.bfloat16)


def dense_hidden(row_block, dense_gate, dense_up):
    return (
        jax.nn.silu(jnp.dot(row_block, dense_gate, preferred_element_type=jnp.float32))
        * jnp.dot(row_block, dense_up, preferred_element_type=jnp.float32)
    ).astype(jnp.bfloat16)


def on_device(
    tokens,
    routes,
    route_logits,
    state_real,
    state_imag,
    gain_in,
    proj_in,
    decay_rate,
    frequency,
    log_step,
    input_real,
    input_imag,
    output_real,
    output_imag,
    skip_gain,
    proj_out,
    gain_mid,
    expert_gate,
    expert_up,
    expert_down,
    dense_gate,
    dense_up,
    dense_down,
    dense_mix,
):
    devices = lax.axis_size(EP)
    own_rows = tokens.shape[0]
    top_count = routes.shape[1]
    capacity = max(2, 2 * own_rows * top_count // devices)
    inputs = tokens.astype(jnp.float32)
    normed = rms_scale(inputs, gain_in).astype(jnp.bfloat16)
    unit_rows = jnp.dot(
        lax.all_gather(normed, EP, axis=0, tiled=True), proj_in, preferred_element_type=jnp.float32
    ).astype(jnp.bfloat16)
    branch, new_real, new_imag = state_step(
        unit_rows,
        state_real,
        state_imag,
        decay_rate,
        frequency,
        log_step,
        input_real,
        input_imag,
        output_real,
        output_imag,
        skip_gain,
    )
    whole_out = lax.all_gather(proj_out, EP, axis=0, tiled=True)
    own_branch = lax.all_to_all(branch, EP, split_axis=0, concat_axis=1, tiled=True)
    mixer_out = jnp.dot(own_branch, whole_out, preferred_element_type=jnp.float32)
    residual = inputs + mixer_out
    mixed = rms_scale(residual, gain_mid).astype(jnp.bfloat16)
    weights = jnp.exp(route_logits)
    weights = weights / jnp.sum(weights, axis=1, keepdims=True)
    whole_rows = lax.all_gather(mixed, EP, axis=0, tiled=True)
    hidden = dense_hidden(whole_rows, dense_gate, dense_up)
    logit_term = jnp.dot(hidden.astype(jnp.float32), dense_mix)
    expert_ids = jnp.arange(devices, dtype=jnp.int32)
    shares = jnp.sum(
        jnp.where(routes[:, :, None] == expert_ids[None, None, :], weights[:, :, None], 0.0), axis=1
    )
    my_shares = lax.all_to_all(shares, EP, split_axis=1, concat_axis=0, tiled=True)[:, 0]
    gate_logit = of_everyone(logit_term, EP)
    marked = (my_shares > 0.0).astype(jnp.int32)
    rank_rows = jnp.cumsum(marked) - 1
    slot_ids = jnp.arange(devices * capacity, dtype=jnp.int32)
    selector = ((rank_rows[None, :] == slot_ids[:, None]) & (marked[None, :] == 1)).astype(
        jnp.bfloat16
    )
    picked = jnp.dot(selector, whole_rows, preferred_element_type=jnp.float32).astype(jnp.bfloat16)
    result = expert_apply(picked, expert_gate[0], expert_up[0], expert_down[0])
    expert_term = my_shares[:, None] * jnp.dot(
        selector.T, result, preferred_element_type=jnp.float32
    )
    gate_weight = jax.nn.sigmoid(gate_logit)
    dense_part = jnp.dot(hidden, dense_down, preferred_element_type=jnp.float32)
    combined = scatter_axes(
        (gate_weight[:, None] * dense_part + expert_term).astype(jnp.bfloat16), EP, (1, 0), 0
    ).astype(jnp.float32)
    layer_out = (residual + combined).astype(jnp.bfloat16)
    return (layer_out, new_real, new_imag)


def solution(mesh):
    split = Mesh(mesh.devices.reshape(mesh.shape["grp"], 16, 2), ("grp", "ep_0", "ep_1"))
    return jax.shard_map(
        on_device,
        mesh=split,
        in_specs=(
            P(GRP_EP, None),
            P(GRP_EP, None),
            P(GRP_EP, None),
            P("grp", EP, None),
            P("grp", EP, None),
            P(),
            P(None, EP),
            P(EP, None),
            P(EP, None),
            P(EP),
            P(EP, None, None),
            P(EP, None, None),
            P(EP, None, None),
            P(EP, None, None),
            P(EP, None),
            P(EP, None),
            P(),
            P(EP, None, None),
            P(EP, None, None),
            P(EP, None, None),
            P(None, EP),
            P(None, EP),
            P(EP, None),
            P(EP),
        ),
        out_specs=(P(GRP_EP, None), P("grp", EP, None), P("grp", EP, None)),
        check_vma=False,
    )
```

profile of v0, /device:TPU:84, one launch (start us, length us, event | category | flops | bytes accessed | tf_op | source)
XLA Modules:
  0.0 369.5 jit_solution(18087104272636381109)
XLA Ops:
  7.2 0.0 copy-start
  7.2 0.1 all-gather.4.cloned.1.call-start
  7.3 1.1 fusion.39
  8.4 1.7 fusion.41
  10.1 0.1 all-gather.4.cloned.1.call-update
  10.2 0.1 all-gather.6.cloned.1.call-start
  10.2 0.7 all-gather.6.cloned.1.call-update
  11.0 0.1 all-gather.8.cloned.1.call-start
  11.1 0.7 exp.23
  11.7 0.8 cosine_multiply_fusion
  12.6 0.0 copy-start.15
  12.6 74.0 %all-gather.4.cloned.1.call-done = bf16[1024,2048]{1,0:T(8,128)(2,1)} async-done(((bf16[32,2048]{1,0:T(8,128)(2,1)}), bf16[1024,2048]{1,0:T(8,128)(2,1)}) %all-gather.4.cloned.1.call-update) | async-done | bytes 4194320 | tf_op jit(solution)/shard_map/all_gather | solution.py:145
  86.5 3.5 convolution_convert_fusion.1
  90.0 0.0 copy-start.4
  90.1 0.3 fusion.58
  90.4 0.4 bitcast_add_fusion
  90.8 0.0 copy-start.2
  90.8 0.0 copy-start.3
  90.8 0.0 copy-start.12
  90.8 0.2 fusion.59
  91.0 0.2 fusion.50
  91.2 0.2 convert_element_type.63
  91.4 0.3 copy.43
  91.7 0.2 reshape.129
  92.0 23.3 %all_to_all.38 = bf16[32,2,512]{2,1,0:T(2,128)(2,1)S(1)} all-to-all(bf16[32,2,512]{2,1,0:T(2,128)(2,1)S(1)} %reshape.129), channel_id=1, replica_groups=mesh['grp'=4,'ep_0'=16,'ep_1'=2] {'ep_0','ep_1'}, dimensions={0} | all-to-all | bytes 131072 | tf_op jit(solution)/shard_map/all_to_all | solution.py:161
  115.2 0.2 reshape.130
  115.4 0.1 copy.44
  115.5 0.3 all_to_all.30
  115.8 41.1 %all-gather.6.cloned.1.call-done = bf16[1024,2048]{1,0:T(8,128)(2,1)} async-done(((bf16[32,2048]{1,0:T(8,128)(2,1)}), bf16[1024,2048]{1,0:T(8,128)(2,1)}) %all-gather.6.cloned.1.call-update) | async-done | bytes 4194320 | tf_op jit(solution)/shard_map/all_gather | solution.py:160
  156.9 3.1 multiply_reduce_fusion
  160.1 0.7 multiply_convert_fusion
  160.9 0.1 all-gather.8.cloned.1.call-update
  161.0 0.1 select_reduce_fusion
  161.1 0.1 copy.46
  161.1 19.3 %all_to_all.39 = f32[32,32,1]{0,2,1:T(1,128)S(1)} all-to-all(f32[32,32,1]{0,2,1:T(1,128)S(1)} %copy.46), channel_id=1, replica_groups=mesh['grp'=4,'ep_0'=16,'ep_1'=2] {'ep_0','ep_1'}, dimensions={1} | all-to-all | bytes 8192 | tf_op jit(solution)/shard_map/all_to_all | solution.py:174
  180.5 0.1 fusion.51
  180.6 0.1 reshape.109
  180.7 0.1 mul.264
  180.7 0.3 reduce-window.9
  181.0 0.1 slice.7
  181.1 0.1 slice_reduce_fusion
  181.2 0.1 add_bitcast_fusion
  181.3 45.6 %all-gather.8.cloned.1.call-done = bf16[1024,2048]{1,0:T(8,128)(2,1)} async-done(((bf16[32,2048]{1,0:T(8,128)(2,1)}), bf16[1024,2048]{1,0:T(8,128)(2,1)}) %all-gather.8.cloned.1.call-update) | async-done | bytes 4194320 | tf_op jit(solution)/shard_map/all_gather | solution.py:167
  226.9 3.7 %fusion.60 = f32[1024,64]{0,1:T(8,128)S(1)} fusion(bf16[1024,2048]{1,0:T(8,128)(2,1)} %all-gather.8.cloned.1.call-done, bf16[2048,64]{0,1:T(8,128)(2,1)S(1)} %copy-done.7), kind=kOutput, calls=%fused_computation.75 | convolution fusion | flops 268435456 | bytes 4718592 | tf_op jit(solution)/shard_map/dot_general | solution.py:107
  230.7 1.4 fusion.27
  232.1 0.1 fusion.55
  232.2 0.7 broadcast_in_dim.10
  233.0 9.0 %all-to-all-start.1 = ((f32[32,1,1024]{2,1,0:T(1,128)}), f32[32,1,1024]{2,1,0:T(1,128)S(1)}, u32[]{:S(2)}, u32[]{:S(2)}) async-start(f32[32,1,1024]{2,1,0:T(1,128)} %broadcast_in_dim.10), calls=%async_computation.1 | async-start | bytes 262144 | tf_op jit(solution)/shard_map/all_to_all | solution.py:16
  242.0 0.2 reduce-scatter.3.cloned.1.call-start
  242.3 3.6 convolution_convert_fusion
  245.9 1.3 fusion.9
  247.2 0.9 copy-done.18
  248.1 1.4 fusion.24
  249.5 4.5 %fusion.61 = f32[1024,2048]{1,0:T(8,128)} fusion(bf16[1024,64]{0,1:T(8,128)(2,1)S(1)} %fusion.27, bf16[64,2048]{1,0:T(8,128)(2,1)S(1)} %copy-done), kind=kOutput, calls=%fused_computation.76 | convolution fusion | flops 268435456 | bytes 8781824 | tf_op jit(solution)/shard_map/dot_general | solution.py:188
  254.0 4.5 %all-to-all-done.1 = f32[32,1,1024]{2,1,0:T(1,128)S(1)} async-done(((f32[32,1,1024]{2,1,0:T(1,128)}), f32[32,1,1024]{2,1,0:T(1,128)S(1)}, u32[]{:S(2)}, u32[]{:S(2)}) %all-to-all-start.1) | async-done | bytes 131104 | tf_op jit(solution)/shard_map/all_to_all | solution.py:16
  258.5 0.1 reduce_sum.47
  258.6 8.6 %add_convert_fusion = bf16[1024,2048]{1,0:T(8,128)(2,1)} fusion(f32[1024,2048]{1,0:T(8,128)} %fusion.61, f32[1024]{0:T(1024)S(1)} %mul.264, f32[1024]{0:T(1024)S(1)} %add_divide_fusion, bf16[256,1024]{1,0:T(8,128)(2,1)S(1)} %fusion.24, bf16[1,1024,2048]{2,1,0:T(8,128)(2,1)} %param.43, s32[1024]{0:T(1024)S(1)} %add_bitcast_fusion, ...), kind=kOutput, calls=%fused_computation | convolution fusion | flops 2156920832 | bytes 17314816 | tf_op jit(solution)/shard_map/dot_general | solution.py:184
  267.2 4.7 %copy.47 = bf16[16,2,32,2048]{3,2,0,1:T(8,128)(2,1)} copy(bf16[16,2,32,2048]{3,2,1,0:T(8,128)(2,1)} %bitcast.98) | data formatting | bytes 8388608 | tf_op jit(solution)/shard_map/reshape;reshape | solution.py:27
  271.9 0.1 reduce-scatter.3.cloned.1.call-update
  272.0 0.1 reduce-scatter.5.cloned.1.call-start
  272.1 15.7 %reduce-scatter.3.cloned.1.call-done = bf16[16,32,2048]{2,1,0:T(8,128)(2,1)} async-done(((bf16[32,32,2048]{2,1,0:T(8,128)(2,1)}), bf16[16,32,2048]{2,1,0:T(8,128)(2,1)}) %reduce-scatter.3.cloned.1.call-update) | async-done | bytes 2097168 | tf_op jit(solution)/shard_map/reduce_scatter | solution.py:31
  287.7 0.1 reduce-scatter.5.cloned.1.call-update
  287.8 73.6 %reduce-scatter.5.cloned.1.call-done = bf16[1,32,2048]{2,1,0:T(8,128)(2,1)} async-done(((bf16[16,32,2048]{2,1,0:T(8,128)(2,1)}), bf16[1,32,2048]{2,1,0:T(8,128)(2,1)}) %reduce-scatter.5.cloned.1.call-update) | async-done | bytes 131088 | tf_op jit(solution)/shard_map/reduce_scatter | solution.py:31
  361.4 1.6 fusion.42
  (41 shorter events, 0.2 us)
Async XLA Ops:
  7.2 242.3 %copy-start = (bf16[64,2048]{1,0:T(8,128)(2,1)S(1)}, bf16[64,2048]{1,0:T(8,128)(2,1)}, u32[]{:S(2)}) copy-start(bf16[64,2048]{1,0:T(8,128)(2,1)} %param.46) | copy-start | bytes 786436
  7.2 82.9 %copy-start.9 = (f32[2,64,16]{1,2,0:T(8,128)S(1)}, f32[2,64,16]{1,2,0:T(8,128)}, u32[]{:S(2)}) copy-start(f32[2,64,16]{1,2,0:T(8,128)} %param.35) | copy-start | bytes 24580
  7.2 83.1 %copy-start.8 = (f32[2,64,16]{1,2,0:T(8,128)S(1)}, f32[2,64,16]{1,2,0:T(8,128)}, u32[]{:S(2)}) copy-start(f32[2,64,16]{1,2,0:T(8,128)} %param.34) | copy-start | bytes 24580
  7.2 83.1 %copy-start.6 = (f32[1024,2,64]{0,2,1:T(8,128)S(1)}, f32[1024,2,64]{0,2,1:T(8,128)}, u32[]{:S(2)}) copy-start(f32[1024,2,64]{0,2,1:T(8,128)} %param.28) | copy-start | bytes 1572868
  7.2 83.1 %copy-start.5 = (f32[1024,2,64]{0,2,1:T(8,128)S(1)}, f32[1024,2,64]{0,2,1:T(8,128)}, u32[]{:S(2)}) copy-start(f32[1024,2,64]{0,2,1:T(8,128)} %param.27) | copy-start | bytes 1572868
  7.2 79.3 %all-gather.4.cloned.1.call-start = ((), (), s32[]{:S(2)}) async-start(), calls=%async_computation.5 | async-start | bytes 4325376 | tf_op jit(solution)/shard_map/all_gather | solution.py:145
  10.2 146.8 %all-gather.6.cloned.1.call-start = ((), (), s32[]{:S(2)}) async-start(), calls=%async_computation.6 | async-start | bytes 4325376 | tf_op jit(solution)/shard_map/all_gather | solution.py:160
  11.0 215.9 %all-gather.8.cloned.1.call-start = ((), (), s32[]{:S(2)}) async-start(), calls=%async_computation.7 | async-start | bytes 4325376 | tf_op jit(solution)/shard_map/all_gather | solution.py:167
  12.5 78.3 %copy-start.11 = (f32[2,16,64]{2,1,0:T(8,128)S(1)}, f32[2,16,64]{2,1,0:T(8,128)}, u32[]{:S(2)}) copy-start(f32[2,16,64]{2,1,0:T(8,128)} %param.36) | copy-start | bytes 24580
  12.5 78.4 %copy-start.10 = (f32[2,16,64]{2,1,0:T(8,128)S(1)}, f32[2,16,64]{2,1,0:T(8,128)}, u32[]{:S(2)}) copy-start(f32[2,16,64]{2,1,0:T(8,128)} %param.37) | copy-start | bytes 24580
  12.6 78.4 %copy-start.15 = (f32[2,16]{1,0:T(2,128)S(1)}, f32[2,16]{1,0:T(2,128)}, u32[]{:S(2)}) copy-start(f32[2,16]{1,0:T(2,128)} %param.38) | copy-start | bytes 388
  90.0 66.9 %copy-start.4 = (bf16[32,2048]{1,0:T(8,128)(2,1)S(1)}, bf16[32,2048]{1,0:T(8,128)(2,1)}, u32[]{:S(2)}) copy-start(bf16[32,2048]{1,0:T(8,128)(2,1)} %param.24) | copy-start | bytes 393220
  90.8 69.3 %copy-start.2 = (f32[1024,2,64]{0,2,1:T(8,128)}, f32[1024,2,64]{0,2,1:T(8,128)S(1)}, u32[]{:S(2)}) copy-start(f32[1024,2,64]{0,2,1:T(8,128)S(1)} %get-tuple-element.3) | copy-start | bytes 1572868
  90.8 69.3 %copy-start.3 = (f32[1024,2,64]{0,2,1:T(8,128)}, f32[1024,2,64]{0,2,1:T(8,128)S(1)}, u32[]{:S(2)}) copy-start(f32[1024,2,64]{0,2,1:T(8,128)S(1)} %get-tuple-element.4) | copy-start | bytes 1572868
  90.8 69.3 %copy-start.12 = (f32[2048]{0:T(1024)S(1)}, f32[2048]{0:T(1024)}, u32[]{:S(2)}) copy-start(f32[2048]{0:T(1024)} %param.40) | copy-start | bytes 24580
  91.0 69.9 %copy-start.13 = (f32[32,4]{0,1:T(4,128)S(1)}, f32[32,4]{0,1:T(4,128)}, u32[]{:S(2)}) copy-start(f32[32,4]{0,1:T(4,128)} %param.26) | copy-start | bytes 1540
  91.0 70.0 %copy-start.14 = (s32[32,4]{0,1:T(4,128)S(1)}, s32[32,4]{0,1:T(4,128)}, u32[]{:S(2)}) copy-start(s32[32,4]{0,1:T(4,128)} %param.25) | copy-start | bytes 1540
  91.0 135.9 %copy-start.7 = (bf16[2048,64]{0,1:T(8,128)(2,1)S(1)}, bf16[2048,64]{0,1:T(8,128)(2,1)}, u32[]{:S(2)}) copy-start(bf16[2048,64]{0,1:T(8,128)(2,1)} %param.44) | copy-start | bytes 786436
  160.1 70.6 %copy-start.19 = (bf16[2048,64]{0,1:T(8,128)(2,1)S(1)}, bf16[2048,64]{0,1:T(8,128)(2,1)}, u32[]{:S(2)}) copy-start(bf16[2048,64]{0,1:T(8,128)(2,1)} %param.45) | copy-start | bytes 786436
  226.9 3.7 %copy-start.1 = (bf16[1024,2048]{1,0:T(8,128)(2,1)S(1)}, bf16[1024,2048]{1,0:T(8,128)(2,1)}, u32[]{:S(2)}) copy-start(bf16[1024,2048]{1,0:T(8,128)(2,1)} %all-gather.8.cloned.1.call-done) | copy-start | bytes 12582916
  230.7 1.4 copy-start.16
  233.0 25.6 %all-to-all-start.1 = ((f32[32,1,1024]{2,1,0:T(1,128)}), f32[32,1,1024]{2,1,0:T(1,128)S(1)}, u32[]{:S(2)}, u32[]{:S(2)}) async-start(f32[32,1,1024]{2,1,0:T(1,128)} %broadcast_in_dim.10), calls=%async_computation.1 | async-start | bytes 262144 | tf_op jit(solution)/shard_map/all_to_all | solution.py:16
  242.0 45.7 %reduce-scatter.3.cloned.1.call-start = ((), (), s32[]{:S(2)}) async-start(), calls=%async_computation.8 | async-start | bytes 6291456 | tf_op jit(solution)/shard_map/reduce_scatter | solution.py:31
  242.3 3.6 copy-start.17
  245.9 2.2 copy-start.18
  272.0 89.4 %reduce-scatter.5.cloned.1.call-start = ((), (), s32[]{:S(2)}) async-start(), calls=%async_computation.9 | async-start | bytes 2228224 | tf_op jit(solution)/shard_map/reduce_scatter | solution.py:31
Sparse Core Ops, SparseCore 0:
  10.3 76.1 all-gather.3
  88.2 68.6 all-gather.5
  161.0 65.8 all-gather.7
  272.1 15.5 reduce-scatter.2
  290.0 71.3 reduce-scatter.4
where the time goes:
time: 370 us; the launch traced here: 369 us
  waiting for transfers between devices  255 us (69%)
  blocking collectives  42.6 us (12%)
  matrix products  32.3 us (9%)
  between operations  14.2 us (4%)
  starting transfers between devices  9.54 us (3%)
  local copies, waits for them, and re-layouts  8.9 us (2%)
  other arithmetic  6.62 us (2%)
    reduce_scatter x2, waiting for transfers between devices, reduced_to_own(): blocks = lax.psum_scatter(blocks, axes[k], scatter_dimension=0, tiled=True)  89.2 us
    all_gather x1, waiting for transfers between devices, on_device(): lax.all_gather(normed, EP, axis=0, tiled=True)  74 us
    all_gather x1, waiting for transfers between devices, on_device(): whole_rows = lax.all_gather(mixed, EP, axis=0, tiled=True)  45.6 us
    all_gather x1, waiting for transfers between devices, on_device(): whole_out = lax.all_gather(proj_out, EP, axis=0, tiled=True)  41.1 us
    all_to_all x1, blocking collectives, on_device(): lax.all_to_all(branch, EP, split_axis=0, concat_axis=1, tiled=True)  23.3 us
    all_to_all x1, blocking collectives, on_device(): lax.all_to_all(shares, EP, split_axis=1, concat_axis=0, tiled=True)[:, 0]  19.3 us
    all_to_all x1, starting transfers between devices, copy_for_each(): lax.all_to_all(jnp.broadcast_to(shard[None], (length, *shard.shape)), axi...  9.04 us
    dot_general x1, matrix products, on_device(): jnp.dot(selector.T, result, preferred_element_type=jnp.float32)  8.6 us
  transfers between devices with their start and end apart: 6, of which 6 were waited for; matrix products, arithmetic and copies ran while one was open for 5% of the time, Pallas kernels for 0%

commit v1 on v0

--- a/solution.py
+++ b/solution.py
@@ -3,6 +3,7 @@
 from jax import lax
 from jax.sharding import Mesh
 from jax.sharding import PartitionSpec as P
+from jax.lax import all_to_all, psum
 
 EP = ("ep_0", "ep_1")
 GRP_EP = ("grp", "ep_0", "ep_1")
@@ -157,7 +158,11 @@
         output_imag,
         skip_gain,
     )
-    whole_out = lax.all_gather(proj_out, EP, axis=0, tiled=True)
+    all_rows = []
+    for _ in range(psum(1, EP)):
+        all_rows.append(proj_out)
+    b_now = all_to_all(jnp.stack(all_rows, 0), EP, 0, 0)
+    whole_out = jnp.concatenate(b_now, 0)
     own_branch = lax.all_to_all(branch, EP, split_axis=0, concat_axis=1, tiled=True)
     mixer_out = jnp.dot(own_branch, whole_out, preferred_element_type=jnp.float32)
     residual = inputs + mixer_out

time: 370 us -> 522 us (1.41)
  waiting for transfers between devices: 255 us -> 404 us
  starting transfers between devices: 9.54 us -> 14.9 us
    all_to_all x0 -> x1, waiting for transfers between devices: none -> 190 us  [on_device(): b_now = all_to_all(jnp.stack(all_rows, 0), EP, 0, 0)]
    all_gather x1 -> x0, waiting for transfers between devices: 41.1 us -> none  [on_device(): whole_out = lax.all_gather(proj_out, EP, axis=0, tiled=True)]
    all_to_all x0 -> x1, starting transfers between devices: none -> 5.8 us  [on_device(): b_now = all_to_all(jnp.stack(all_rows, 0), EP, 0, 0)]
  transfers between devices with their start and end apart: 6 -> 6, of which waited for: 6 -> 6; matrix products, arithmetic and copies ran while one was open for 5% -> 3% of each run, Pallas kernels for 0% -> 0%
where the time goes in v1:
time: 522 us; the launch traced here: 521 us
  waiting for transfers between devices  404 us (77%)
  blocking collectives  38.2 us (7%)
  matrix products  32.4 us (6%)
  starting transfers between devices  14.9 us (3%)
  between operations  14.2 us (3%)
  local copies, waits for them, and re-layouts  11 us (2%)
  other arithmetic  6.62 us (1%)
    all_to_all x1, waiting for transfers between devices, on_device(): b_now = all_to_all(jnp.stack(all_rows, 0), EP, 0, 0)  190 us
    reduce_scatter x2, waiting for transfers between devices, reduced_to_own(): blocks = lax.psum_scatter(blocks, axes[k], scatter_dimension=0, tiled=True)  89.1 us
    all_gather x1, waiting for transfers between devices, on_device(): lax.all_gather(normed, EP, axis=0, tiled=True)  74.8 us
    all_gather x1, waiting for transfers between devices, on_device(): whole_rows = lax.all_gather(mixed, EP, axis=0, tiled=True)  45.1 us
    all_to_all x1, blocking collectives, on_device(): lax.all_to_all(branch, EP, split_axis=0, concat_axis=1, tiled=True)  22.6 us
    all_to_all x1, blocking collectives, on_device(): lax.all_to_all(shares, EP, split_axis=1, concat_axis=0, tiled=True)[:, 0]  15.6 us
  transfers between devices with their start and end apart: 6, of which 6 were waited for; matrix products, arithmetic and copies ran while one was open for 3% of the time, Pallas kernels for 0%

profile of v1, /device:TPU:84, one launch (start us, length us, event | category | flops | bytes accessed | tf_op | source)
XLA Modules:
  0.0 521.5 jit_solution(7528500858881764716)
XLA Ops:
  7.2 0.0 copy-start
  7.2 0.1 all-gather.3.cloned.1.call-start
  7.3 1.1 fusion.40
  8.4 1.7 fusion.42
  10.1 0.1 all-gather.3.cloned.1.call-update
  10.2 0.7 exp.23
  10.8 0.8 cosine_multiply_fusion
  11.6 0.0 copy-start.12
  11.7 0.0 copy-start.11
  11.7 74.8 %all-gather.3.cloned.1.call-done = bf16[1024,2048]{1,0:T(8,128)(2,1)} async-done(((bf16[32,2048]{1,0:T(8,128)(2,1)}), bf16[1024,2048]{1,0:T(8,128)(2,1)}) %all-gather.3.cloned.1.call-update) | async-done | bytes 4194320 | tf_op jit(solution)/shard_map/all_gather | solution.py:146
  86.5 3.5 convolution_convert_fusion.1
  90.0 0.0 copy-start.8
  90.1 0.3 fusion.60
  90.4 0.4 bitcast_add_fusion
  90.8 0.0 copy-start.2
  90.8 0.0 copy-start.3
  90.8 0.2 fusion.61
  91.0 0.2 fusion.52
  91.2 0.2 convert_element_type.63
  91.4 0.3 copy.42
  91.7 0.2 reshape.133
  91.9 22.6 %all_to_all.40 = bf16[32,2,512]{2,1,0:T(2,128)(2,1)S(1)} all-to-all(bf16[32,2,512]{2,1,0:T(2,128)(2,1)S(1)} %reshape.133), channel_id=1, replica_groups=mesh['grp'=4,'ep_0'=16,'ep_1'=2] {'ep_0','ep_1'}, dimensions={0} | all-to-all | bytes 131072 | tf_op jit(solution)/shard_map/all_to_all | solution.py:166
  114.5 2.5 stack.2
  117.0 5.8 %all-to-all-start.1 = ((bf16[32,32,2048]{2,1,0:T(8,128)(2,1)}), bf16[32,32,2048]{2,1,0:T(8,128)(2,1)}, u32[]{:S(2)}, u32[]{:S(2)}) async-start(bf16[32,32,2048]{2,1,0:T(8,128)(2,1)} %stack.2), calls=%async_computation.1 | async-start | bytes 8388608 | tf_op jit(solution)/shard_map/all_to_all | solution.py:164
  122.8 0.0 copy-start.13
  122.9 0.0 copy-start.14
  122.9 0.1 all-gather.5.cloned.1.call-start
  123.0 0.2 reshape.134
  123.2 190.3 %all-to-all-done.1 = bf16[32,32,2048]{2,1,0:T(8,128)(2,1)} async-done(((bf16[32,32,2048]{2,1,0:T(8,128)(2,1)}), bf16[32,32,2048]{2,1,0:T(8,128)(2,1)}, u32[]{:S(2)}, u32[]{:S(2)}) %all-to-all-start.1) | async-done | bytes 4194336 | tf_op jit(solution)/shard_map/all_to_all | solution.py:164
  313.5 3.3 multiply_reduce_fusion
  316.8 0.7 multiply_convert_fusion
  317.6 0.1 all-gather.5.cloned.1.call-update
  317.7 0.1 select_reduce_fusion
  317.8 0.1 copy.44
  317.9 15.6 %all_to_all.41 = f32[32,32,1]{0,2,1:T(1,128)S(1)} all-to-all(f32[32,32,1]{0,2,1:T(1,128)S(1)} %copy.44), channel_id=1, replica_groups=mesh['grp'=4,'ep_0'=16,'ep_1'=2] {'ep_0','ep_1'}, dimensions={1} | all-to-all | bytes 8192 | tf_op jit(solution)/shard_map/all_to_all | solution.py:179
  333.5 0.1 fusion.53
  333.6 0.1 reshape.112
  333.7 0.1 mul.264
  333.7 0.3 reduce-window.9
  334.0 0.1 slice.7
  334.1 0.1 slice_reduce_fusion
  334.2 0.1 add_bitcast_fusion
  334.3 45.1 %all-gather.5.cloned.1.call-done = bf16[1024,2048]{1,0:T(8,128)(2,1)} async-done(((bf16[32,2048]{1,0:T(8,128)(2,1)}), bf16[1024,2048]{1,0:T(8,128)(2,1)}) %all-gather.5.cloned.1.call-update) | async-done | bytes 4194320 | tf_op jit(solution)/shard_map/all_gather | solution.py:172
  379.4 3.7 fusion.62
  383.2 1.4 fusion.28
  384.6 0.1 fusion.57
  384.7 0.7 broadcast_in_dim.10
  385.4 8.6 %all-to-all-start.2 = ((f32[32,1,1024]{2,1,0:T(1,128)}), f32[32,1,1024]{2,1,0:T(1,128)S(1)}, u32[]{:S(2)}, u32[]{:S(2)}) async-start(f32[32,1,1024]{2,1,0:T(1,128)} %broadcast_in_dim.10), calls=%async_computation.2 | async-start | bytes 262144 | tf_op jit(solution)/shard_map/all_to_all | solution.py:17
  394.1 0.2 reduce-scatter.3.cloned.1.call-start
  394.3 3.6 convolution_convert_fusion
  398.0 1.3 fusion.10
  399.2 0.9 copy-done.19
  400.1 1.4 fusion.25
  401.6 4.5 fusion.63
  406.1 4.5 all-to-all-done.2
  410.6 0.1 reduce_sum.47
  410.7 8.6 %add_convert_fusion = bf16[1024,2048]{1,0:T(8,128)(2,1)} fusion(f32[1024,2048]{1,0:T(8,128)} %fusion.63, f32[1024]{0:T(1024)S(1)} %mul.264, f32[1024]{0:T(1024)S(1)} %add_divide_fusion, bf16[256,1024]{1,0:T(8,128)(2,1)S(1)} %fusion.25, bf16[1,1024,2048]{2,1,0:T(8,128)(2,1)} %param.43, s32[1024]{0:T(1024)S(1)} %add_bitcast_fusion, ...), kind=kOutput, calls=%fused_computation | convolution fusion | flops 2156920832 | bytes 17314816 | tf_op jit(solution)/shard_map/dot_general | solution.py:189
  419.3 4.7 copy.45
  424.0 0.1 reduce-scatter.3.cloned.1.call-update
  424.0 0.1 reduce-scatter.5.cloned.1.call-start
  424.1 15.6 %reduce-scatter.3.cloned.1.call-done = bf16[16,32,2048]{2,1,0:T(8,128)(2,1)} async-done(((bf16[32,32,2048]{2,1,0:T(8,128)(2,1)}), bf16[16,32,2048]{2,1,0:T(8,128)(2,1)}) %reduce-scatter.3.cloned.1.call-update) | async-done | bytes 2097168 | tf_op jit(solution)/shard_map/reduce_scatter | solution.py:32
  439.7 0.1 reduce-scatter.5.cloned.1.call-update
  439.8 73.5 %reduce-scatter.5.cloned.1.call-done = bf16[1,32,2048]{2,1,0:T(8,128)(2,1)} async-done(((bf16[16,32,2048]{2,1,0:T(8,128)(2,1)}), bf16[1,32,2048]{2,1,0:T(8,128)(2,1)}) %reduce-scatter.5.cloned.1.call-update) | async-done | bytes 131088 | tf_op jit(solution)/shard_map/reduce_scatter | solution.py:32
  513.3 1.6 fusion.43
  (41 shorter events, 0.2 us)
Async XLA Ops:
  7.2 394.4 %copy-start = (bf16[64,2048]{1,0:T(8,128)(2,1)S(1)}, bf16[64,2048]{1,0:T(8,128)(2,1)}, u32[]{:S(2)}) copy-start(bf16[64,2048]{1,0:T(8,128)(2,1)} %param.46) | copy-start | bytes 786436
  7.2 82.9 %copy-start.10 = (f32[2,64,16]{1,2,0:T(8,128)S(1)}, f32[2,64,16]{1,2,0:T(8,128)}, u32[]{:S(2)}) copy-start(f32[2,64,16]{1,2,0:T(8,128)} %param.35) | copy-start | bytes 24580
  7.2 83.1 %copy-start.9 = (f32[2,64,16]{1,2,0:T(8,128)S(1)}, f32[2,64,16]{1,2,0:T(8,128)}, u32[]{:S(2)}) copy-start(f32[2,64,16]{1,2,0:T(8,128)} %param.34) | copy-start | bytes 24580
  7.2 83.1 %copy-start.6 = (f32[1024,2,64]{0,2,1:T(8,128)S(1)}, f32[1024,2,64]{0,2,1:T(8,128)}, u32[]{:S(2)}) copy-start(f32[1024,2,64]{0,2,1:T(8,128)} %param.28) | copy-start | bytes 1572868
  7.2 83.1 %copy-start.5 = (f32[1024,2,64]{0,2,1:T(8,128)S(1)}, f32[1024,2,64]{0,2,1:T(8,128)}, u32[]{:S(2)}) copy-start(f32[1024,2,64]{0,2,1:T(8,128)} %param.27) | copy-start | bytes 1572868
  7.2 79.3 %all-gather.3.cloned.1.call-start = ((), (), s32[]{:S(2)}) async-start(), calls=%async_computation.6 | async-start | bytes 4325376 | tf_op jit(solution)/shard_map/all_gather | solution.py:146
  11.6 79.2 %copy-start.12 = (f32[2,16,64]{2,1,0:T(8,128)S(1)}, f32[2,16,64]{2,1,0:T(8,128)}, u32[]{:S(2)}) copy-start(f32[2,16,64]{2,1,0:T(8,128)} %param.36) | copy-start | bytes 24580
  11.7 79.3 %copy-start.11 = (f32[2,16,64]{2,1,0:T(8,128)S(1)}, f32[2,16,64]{2,1,0:T(8,128)}, u32[]{:S(2)}) copy-start(f32[2,16,64]{2,1,0:T(8,128)} %param.37) | copy-start | bytes 24580
  11.7 79.3 %copy-start.16 = (f32[2,16]{1,0:T(2,128)S(1)}, f32[2,16]{1,0:T(2,128)}, u32[]{:S(2)}) copy-start(f32[2,16]{1,0:T(2,128)} %param.38) | copy-start | bytes 388
  90.0 24.5 %copy-start.8 = (bf16[32,2048]{1,0:T(8,128)(2,1)S(1)}, bf16[32,2048]{1,0:T(8,128)(2,1)}, u32[]{:S(2)}) copy-start(bf16[32,2048]{1,0:T(8,128)(2,1)} %param.39) | copy-start | bytes 393220
  90.8 26.3 %copy-start.2 = (f32[1024,2,64]{0,2,1:T(8,128)}, f32[1024,2,64]{0,2,1:T(8,128)S(1)}, u32[]{:S(2)}) copy-start(f32[1024,2,64]{0,2,1:T(8,128)S(1)} %get-tuple-element.3) | copy-start | bytes 1572868
  90.8 26.3 %copy-start.3 = (f32[1024,2,64]{0,2,1:T(8,128)}, f32[1024,2,64]{0,2,1:T(8,128)S(1)}, u32[]{:S(2)}) copy-start(f32[1024,2,64]{0,2,1:T(8,128)S(1)} %get-tuple-element.4) | copy-start | bytes 1572868
  117.0 196.4 %copy-start.4 = (bf16[32,2048]{1,0:T(8,128)(2,1)S(1)}, bf16[32,2048]{1,0:T(8,128)(2,1)}, u32[]{:S(2)}) copy-start(bf16[32,2048]{1,0:T(8,128)(2,1)} %param.24) | copy-start | bytes 393220
  117.0 196.4 %all-to-all-start.1 = ((bf16[32,32,2048]{2,1,0:T(8,128)(2,1)}), bf16[32,32,2048]{2,1,0:T(8,128)(2,1)}, u32[]{:S(2)}, u32[]{:S(2)}) async-start(bf16[32,32,2048]{2,1,0:T(8,128)(2,1)} %stack.2), calls=%async_computation.1 | async-start | bytes 8388608 | tf_op jit(solution)/shard_map/all_to_all | solution.py:164
  122.8 194.0 %copy-start.13 = (f32[2048]{0:T(1024)S(1)}, f32[2048]{0:T(1024)}, u32[]{:S(2)}) copy-start(f32[2048]{0:T(1024)} %param.40) | copy-start | bytes 24580
  122.9 194.8 %copy-start.14 = (f32[32,4]{0,1:T(4,128)S(1)}, f32[32,4]{0,1:T(4,128)}, u32[]{:S(2)}) copy-start(f32[32,4]{0,1:T(4,128)} %param.26) | copy-start | bytes 1540
  122.9 194.8 %copy-start.15 = (s32[32,4]{0,1:T(4,128)S(1)}, s32[32,4]{0,1:T(4,128)}, u32[]{:S(2)}) copy-start(s32[32,4]{0,1:T(4,128)} %param.25) | copy-start | bytes 1540
  122.9 256.5 %copy-start.7 = (bf16[2048,64]{0,1:T(8,128)(2,1)S(1)}, bf16[2048,64]{0,1:T(8,128)(2,1)}, u32[]{:S(2)}) copy-start(bf16[2048,64]{0,1:T(8,128)(2,1)} %param.44) | copy-start | bytes 786436
  122.9 256.5 %all-gather.5.cloned.1.call-start = ((), (), s32[]{:S(2)}) async-start(), calls=%async_computation.7 | async-start | bytes 4325376 | tf_op jit(solution)/shard_map/all_gather | solution.py:172
  316.8 66.4 %copy-start.20 = (bf16[2048,64]{0,1:T(8,128)(2,1)S(1)}, bf16[2048,64]{0,1:T(8,128)(2,1)}, u32[]{:S(2)}) copy-start(bf16[2048,64]{0,1:T(8,128)(2,1)} %param.45) | copy-start | bytes 786436
  379.4 3.7 copy-start.1
  383.2 1.4 copy-start.17
  385.4 25.1 %all-to-all-start.2 = ((f32[32,1,1024]{2,1,0:T(1,128)}), f32[32,1,1024]{2,1,0:T(1,128)S(1)}, u32[]{:S(2)}, u32[]{:S(2)}) async-start(f32[32,1,1024]{2,1,0:T(1,128)} %broadcast_in_dim.10), calls=%async_computation.2 | async-start | bytes 262144 | tf_op jit(solution)/shard_map/all_to_all | solution.py:17
  394.1 45.6 %reduce-scatter.3.cloned.1.call-start = ((), (), s32[]{:S(2)}) async-start(), calls=%async_computation.8 | async-start | bytes 6291456 | tf_op jit(solution)/shard_map/reduce_scatter | solution.py:32
  394.3 3.6 copy-start.18
  397.9 2.2 copy-start.19
  424.0 89.3 %reduce-scatter.5.cloned.1.call-start = ((), (), s32[]{:S(2)}) async-start(), calls=%async_computation.9 | async-start | bytes 2228224 | tf_op jit(solution)/shard_map/reduce_scatter | solution.py:32
Sparse Core Ops, SparseCore 0:
  10.3 76.1 all-gather.2
  317.7 61.6 all-gather.4
  424.2 15.5 reduce-scatter.2
  442.0 71.2 reduce-scatter.4
